TPU v7x, 32 devices: a whole 2x2x4 slice. The times are simulated.
32 devices in a mesh: ra: 8 (over z, y), cb: 4 (over x, core).
Axes of the slice: x: 2, y: 2, z: 4, core: 2. Of those that a mesh axis runs over, the one named last changes fastest.
Arguments:
- stream: bfloat16 [64, 1024], P(None, 'ra'), may hold values from -24 to 24, as said below
- gain_first: float32 [1024], P('ra'), may hold values from 0.5 to 1.5
- up_first: float32 [1024, 4096], P('ra', 'cb'), may hold values from -0.1875 to 0.1875
- down_first: float32 [4096, 1024], P('cb', 'ra'), may hold values from -0.09375 to 0.09375
- gain_second: float32 [1024], P('ra'), may hold values from 0.5 to 1.5
- up_second: float32 [1024, 4096], P('ra', 'cb'), may hold values from -0.1875 to 0.1875
- down_second: float32 [4096, 1024], P('cb', 'ra'), may hold values from -0.09375 to 0.09375
Outputs:
- read: bfloat16 [64, 1024], P(None, 'ra')
Inputs may be any that keep to these rules, and one draw needn't show every extreme that they name: stream is of order one, and in each token one aligned block of 128 features is four times larger than the rest.
All inputs are finite; a program needn't handle non-finite values.
Results may differ from a plain program's by a relative error of at most 0.025.
Values may be sent and summed in bfloat16 or wider, within the bound.
A program may use at most 64 MiB of HBM per device.

v0:
```python
import jax
import jax.numpy as jnp
from jax import lax
from jax.sharding import PartitionSpec as P

D = 1024


EPS = 1e-06
RESIDUAL = 0.25


def sublayer(stream, norm_gain, w_up, w_down):
    floated = stream.astype(jnp.float32)
    own_squares = jnp.sum(floated * floated, axis=1, keepdims=True)
    squares = lax.psum(own_squares, "ra")
    factor = lax.rsqrt(squares / D + EPS)
    normed = (floated * factor * norm_gain.astype(jnp.float32)[None, :]).astype(jnp.bfloat16)
    up_bf = w_up.astype(jnp.bfloat16)
    down_bf = w_down.astype(jnp.bfloat16)
    partial_value = jnp.dot(normed, up_bf, preferred_element_type=jnp.float32)
    preact = lax.psum(partial_value, "ra")
    activated = jnp.square(jax.nn.relu(preact)).astype(jnp.bfloat16)
    down_part = jnp.dot(activated, down_bf, preferred_element_type=jnp.float32)
    branch = lax.psum(down_part.astype(jnp.bfloat16), "cb").astype(jnp.float32)
    return (RESIDUAL * floated + branch).astype(jnp.bfloat16)


def local(stream, gain_first, up_first, down_first, gain_second, up_second, down_second):
    middle = sublayer(stream, gain_first, up_first, down_first)
    return sublayer(middle, gain_second, up_second, down_second)


def solution(mesh):
    return jax.shard_map(
        local,
        mesh=mesh,
        in_specs=(
            P(None, "ra"),
            P("ra"),
            P("ra", "cb"),
            P("cb", "ra"),
            P("ra"),
            P("ra", "cb"),
            P("cb", "ra"),
        ),
        out_specs=P(None, "ra"),
        check_vma=False,
    )
```

profile of v0, /device:TPU:0, one launch (start us, length us, event | category | flops | bytes accessed | tf_op | source)
XLA Modules:
  0.0 222.2 jit_solution(7013383935762173612)
XLA Ops:
  6.5 0.0 copy-start.3
  6.5 0.0 all-reduce.3.cloned.1.call-start
  6.5 0.9 fusion.10
  7.4 23.2 %psum.42 = f32[64,1]{0,1:T(1,128)S(1)} all-reduce(f32[64,1]{0,1:T(1,128)S(1)} %bitcast.7), channel_id=1, replica_groups=mesh['ra'=8,'cb'=4] {'ra'}, use_global_device_ids=true, to_apply=%region_1.0 | all-reduce | flops 64 | bytes 512 | tf_op jit(solution)/shard_map/psum | solution.py:16
  30.6 0.0 copy-start.4
  30.6 0.0 copy-done.3
  30.6 0.6 copy-done.4
  31.3 0.0 copy-start.1
  31.3 2.0 fusion.4
  33.3 0.0 copy-start
  33.3 0.0 all-reduce.3.cloned.1.call-update
  33.3 0.0 all-reduce.5.cloned.1.call-start
  33.4 68.7 %all-reduce.3.cloned.1.call-done = f32[64,1024]{1,0:T(8,128)} async-done(((f32[64,1024]{1,0:T(8,128)}), f32[64,1024]{1,0:T(8,128)}) %all-reduce.3.cloned.1.call-update) | async-done | bytes 262160 | tf_op jit(solution)/shard_map/psum | solution.py:22
  102.0 0.0 copy-done.1
  102.0 1.1 convolution_convert_fusion.1
  103.2 10.1 %psum.44 = bf16[64,128]{1,0:T(8,128)(2,1)S(1)} all-reduce(bf16[64,128]{1,0:T(8,128)(2,1)S(1)} %convolution_convert_fusion.1), channel_id=1, replica_groups=mesh['ra'=8,'cb'=4] {'cb'}, use_global_device_ids=true, to_apply=%region_3.4 | all-reduce | flops 8192 | bytes 32768 | tf_op jit(solution)/shard_map/psum | solution.py:25
  113.3 0.1 fusion.15
  113.4 19.6 %psum.45 = f32[64,1]{0,1:T(1,128)S(1)} all-reduce(f32[64,1]{0,1:T(1,128)S(1)} %bitcast.6), channel_id=1, replica_groups=mesh['ra'=8,'cb'=4] {'ra'}, use_global_device_ids=true, to_apply=%region_5.6 | all-reduce | flops 64 | bytes 512 | tf_op jit(solution)/shard_map/psum | solution.py:16
  133.0 0.0 copy-start.5
  133.1 0.0 copy-done
  133.1 0.6 copy-done.5
  133.7 0.0 copy-start.2
  133.7 0.9 fusion.1
  134.6 0.0 all-reduce.5.cloned.1.call-update
  134.7 68.8 %all-reduce.5.cloned.1.call-done = f32[64,1024]{1,0:T(8,128)} async-done(((f32[64,1024]{1,0:T(8,128)}), f32[64,1024]{1,0:T(8,128)}) %all-reduce.5.cloned.1.call-update) | async-done | bytes 262160 | tf_op jit(solution)/shard_map/psum | solution.py:22
  203.5 0.0 copy-done.2
  203.5 1.1 convolution_convert_fusion
  204.6 10.1 %psum.47 = bf16[64,128]{1,0:T(8,128)(2,1)S(1)} all-reduce(bf16[64,128]{1,0:T(8,128)(2,1)S(1)} %convolution_convert_fusion), channel_id=1, replica_groups=mesh['ra'=8,'cb'=4] {'cb'}, use_global_device_ids=true, to_apply=%region_7.8 | all-reduce | flops 8192 | bytes 32768 | tf_op jit(solution)/shard_map/psum | solution.py:25
  214.7 0.6 fusion.14
  (2 shorter events, 0.0 us)
Async XLA Ops:
  6.5 24.1 %copy-start.3 = (bf16[64,128]{1,0:T(8,128)(2,1)S(1)}, bf16[64,128]{1,0:T(8,128)(2,1)}, u32[]{:S(2)}) copy-start(bf16[64,128]{1,0:T(8,128)(2,1)} %param.7) | copy-start | bytes 49156
  6.5 95.5 %all-reduce.3.cloned.1.call-start = ((), (), s32[]{:S(2)}) async-start(), calls=%async_computation | async-start | bytes 524288 | tf_op jit(solution)/shard_map/psum | solution.py:22
  30.6 0.7 copy-start.4
  31.3 70.8 %copy-start.1 = (f32[1024,128]{1,0:T(8,128)S(1)}, f32[1024,128]{1,0:T(8,128)}, u32[]{:S(2)}) copy-start(f32[1024,128]{1,0:T(8,128)} %param.10) | copy-start | bytes 1572868
  33.3 99.7 %copy-start = (f32[128,1024]{1,0:T(8,128)S(1)}, f32[128,1024]{1,0:T(8,128)}, u32[]{:S(2)}) copy-start(f32[128,1024]{1,0:T(8,128)} %param.12) | copy-start | bytes 1572868
  33.3 170.1 %all-reduce.5.cloned.1.call-start = ((), (), s32[]{:S(2)}) async-start(), calls=%async_computation.1 | async-start | bytes 524288 | tf_op jit(solution)/shard_map/psum | solution.py:22
  133.0 0.7 copy-start.5
  133.7 69.8 %copy-start.2 = (f32[1024,128]{1,0:T(8,128)S(1)}, f32[1024,128]{1,0:T(8,128)}, u32[]{:S(2)}) copy-start(f32[1024,128]{1,0:T(8,128)} %param.13) | copy-start | bytes 1572868
Sparse Core Ops, SparseCore 0:
  33.5 68.5 all-reduce.2
  134.8 68.6 all-reduce.4
where the time goes:
time: 223 us; the launch traced here: 222 us
  waiting for transfers between devices  138 us (62%)
  blocking collectives  63.1 us (28%)
  between operations  13.4 us (6%)
  matrix products  5.2 us (2%)
    psum x2, waiting for transfers between devices, sublayer(): preact = lax.psum(partial_value, 'ra')  137 us
    psum x2, blocking collectives, sublayer(): squares = lax.psum(own_squares, 'ra')  42.8 us
    psum x2, blocking collectives, sublayer(): branch = lax.psum(down_part.astype(jnp.bfloat16), 'cb').astype(jnp.float32)  20.2 us
  transfers between devices with their start and end apart: 2, of which 2 were waited for; matrix products, arithmetic and copies ran while one was open for 0% of the time, Pallas kernels for 0%

commit v1 on v0

v1 whole, which is shorter than its diff:
```python
import functools

import jax
import jax.numpy as jnp
from jax import lax
from jax.experimental import pallas as pl
from jax.experimental.pallas import tpu as pltpu
from jax.sharding import PartitionSpec as P

EPS = 1e-06
RESIDUAL = 0.25
LANES = 128
ROWS = 8
MESH = pl.DeviceIdType.MESH
F32 = jnp.float32
BF16 = jnp.bfloat16


def kernel(
    n, m, width,
    stream_hbm, gain1_hbm, up1_hbm, down1_hbm, gain2_hbm, up2_hbm, down2_hbm,
    out_ref,
    stream_v, gain_v, up_v, down_v, down_b,
    part_out, part_in, sq_out, sq_in, act, branch_in,
    load_sem, part_ss, part_rs, sq_ss, sq_rs, act_ss, act_rs, br_ss, br_rs,
):
    ra = lax.axis_index("ra")
    cb = lax.axis_index("cb")
    tokens = stream_v.shape[0]
    block = part_out.shape[-1]

    def ra_peer(step):
        return lax.rem(ra + step, n)

    def cb_peer(step):
        return lax.rem(cb + step, m)

    loads = [
        pltpu.make_async_copy(src, dst, load_sem.at[i])
        for i, (src, dst) in enumerate((
            (stream_hbm, stream_v),
            (gain1_hbm, gain_v.at[0]),
            (up1_hbm, up_v.at[0]),
            (down1_hbm, down_v.at[0]),
            (gain2_hbm, gain_v.at[1]),
            (up2_hbm, up_v.at[1]),
            (down2_hbm, down_v.at[1]),
        ))
    ]
    barrier = pltpu.get_barrier_semaphore()
    for step in range(1, n):
        pl.semaphore_signal(barrier, inc=1, device_id={"ra": ra_peer(step)}, device_id_type=MESH)
    for step in range(1, m):
        pl.semaphore_signal(barrier, inc=1, device_id={"cb": cb_peer(step)}, device_id_type=MESH)
    for load in loads:
        load.start()

    def to_ra(src, dst, send, recv, peer):
        return pltpu.make_async_remote_copy(
            src_ref=src, dst_ref=dst, send_sem=send, recv_sem=recv,
            device_id={"ra": peer}, device_id_type=MESH,
        )

    def to_cb(src, dst, send, recv, peer):
        return pltpu.make_async_remote_copy(
            src_ref=src, dst_ref=dst, send_sem=send, recv_sem=recv,
            device_id={"cb": peer}, device_id_type=MESH,
        )

    sends = []
    for load in loads[:2]:
        load.wait()
    floated = stream_v[...].astype(F32)
    result = None
    for layer in range(2):
        scaled = (floated * gain_v[layer]).astype(BF16)
        loads[2 + 3 * layer].wait()
        partial = jnp.dot(scaled, up_v[layer].astype(BF16), preferred_element_type=F32)
        for j in range(n):
            part_out[layer, j] = partial[:, j * block:(j + 1) * block].astype(BF16)
        own = jnp.sum(floated * floated, axis=1, keepdims=True)
        sq_out[layer] = jnp.broadcast_to(own, (tokens, LANES)).T[:ROWS]
        if layer == 0:
            pl.semaphore_wait(barrier, n + m - 2)
        copies = []
        for step in range(1, n):
            peer = ra_peer(step)
            copies.append(to_ra(
                part_out.at[layer, peer], part_in.at[layer, ra],
                part_ss.at[layer, peer], part_rs.at[layer, ra], peer))
        for step in range(1, n):
            peer = ra_peer(step)
            copies.append(to_ra(
                sq_out.at[layer], sq_in.at[layer, ra],
                sq_ss.at[layer, peer], sq_rs.at[layer, ra], peer))
        for copy in copies:
            copy.start()
        sends += copies

        loads[3 + 3 * layer].wait()
        for j in range(n):
            down_b[layer, j] = down_v[layer, j * block:(j + 1) * block, :].astype(BF16)

        preact = part_out[layer, ra].astype(F32)
        for step in range(1, n):
            peer = ra_peer(step)
            to_ra(part_out.at[layer, peer], part_in.at[layer, peer],
                  part_ss.at[layer, peer], part_rs.at[layer, peer], peer).wait_recv()
            preact += part_in[layer, peer].astype(F32)
        positive = jnp.maximum(preact, 0.0)
        act[layer, ra] = (positive * positive).astype(BF16)

        copies = []
        for step in range(1, n):
            peer = ra_peer(step)
            copies.append(to_ra(
                act.at[layer, ra], act.at[layer, ra],
                act_ss.at[layer, peer], act_rs.at[layer, ra], peer))
        for copy in copies:
            copy.start()
        sends += copies

        squares = sq_out[layer]
        for step in range(1, n):
            peer = ra_peer(step)
            to_ra(sq_out.at[layer], sq_in.at[layer, peer],
                  sq_ss.at[layer, peer], sq_rs.at[layer, peer], peer).wait_recv()
            squares += sq_in[layer, peer]
        factor = 1.0 / (squares / width + EPS)
        scale = jnp.broadcast_to(factor[:1], (LANES, tokens)).T[:, :1]

        total = jnp.dot(act[layer, ra], down_b[layer, ra], preferred_element_type=F32)
        for step in range(1, n):
            peer = ra_peer(step)
            to_ra(act.at[layer, peer], act.at[layer, peer],
                  act_ss.at[layer, peer], act_rs.at[layer, peer], peer).wait_recv()
            total += jnp.dot(act[layer, peer], down_b[layer, peer], preferred_element_type=F32)

        branch_in[layer, cb] = (total * scale).astype(BF16)
        copies = []
        for step in range(1, m):
            peer = cb_peer(step)
            copies.append(to_cb(
                branch_in.at[layer, cb], branch_in.at[layer, cb],
                br_ss.at[layer, peer], br_rs.at[layer, cb], peer))
        for copy in copies:
            copy.start()
        sends += copies
        if layer == 0:
            loads[4].wait()
        for step in range(1, m):
            peer = cb_peer(step)
            to_cb(branch_in.at[layer, peer], branch_in.at[layer, peer],
                  br_ss.at[layer, peer], br_rs.at[layer, peer], peer).wait_recv()
        branch = branch_in[layer, 0].astype(F32)
        for j in range(1, m):
            branch += branch_in[layer, j].astype(F32)
        result = (RESIDUAL * floated + branch).astype(BF16)
        floated = result.astype(F32)
    out_ref[...] = result
    for copy in sends:
        copy.wait_send()


def local(n, m, stream, gain_first, up_first, down_first, gain_second, up_second, down_second):
    tokens, cols = stream.shape
    hidden = up_first.shape[1]
    block = hidden // n
    dma = pltpu.SemaphoreType.DMA
    return pl.pallas_call(
        functools.partial(kernel, n, m, cols * n),
        out_shape=jax.ShapeDtypeStruct((tokens, cols), BF16),
        in_specs=[pl.BlockSpec(memory_space=pl.ANY)] * 7,
        out_specs=pl.BlockSpec(memory_space=pltpu.VMEM),
        scratch_shapes=[
            pltpu.VMEM((tokens, cols), BF16),
            pltpu.VMEM((2, 1, cols), F32),
            pltpu.VMEM((2, cols, hidden), F32),
            pltpu.VMEM((2, hidden, cols), F32),
            pltpu.VMEM((2, n, block, cols), BF16),
            pltpu.VMEM((2, n, tokens, block), BF16),
            pltpu.VMEM((2, n, tokens, block), BF16),
            pltpu.VMEM((2, ROWS, tokens), F32),
            pltpu.VMEM((2, n, ROWS, tokens), F32),
            pltpu.VMEM((2, n, tokens, block), BF16),
            pltpu.VMEM((2, m, tokens, cols), BF16),
            dma((7,)),
            dma((2, n)), dma((2, n)),
            dma((2, n)), dma((2, n)),
            dma((2, n)), dma((2, n)),
            dma((2, m)), dma((2, m)),
        ],
        compiler_params=pltpu.CompilerParams(
            collective_id=0, has_side_effects=True
        ),
    )(
        stream, gain_first.reshape(1, cols), up_first, down_first,
        gain_second.reshape(1, cols), up_second, down_second,
    )


def solution(mesh):
    return jax.shard_map(
        functools.partial(local, mesh.shape["ra"], mesh.shape["cb"]),
        mesh=mesh,
        in_specs=(
            P(None, "ra"),
            P("ra"),
            P("ra", "cb"),
            P("cb", "ra"),
            P("ra"),
            P("ra", "cb"),
            P("cb", "ra"),
        ),
        out_specs=P(None, "ra"),
        check_vma=False,
    )
```

time: 223 us -> 36.7 us (0.16)
  waiting for transfers between devices: 138 us -> 0 us
  blocking collectives: 63.1 us -> 0 us
  Pallas kernels: 0 us -> 35.1 us
  between operations: 13.4 us -> 0.01 us
  matrix products: 5.2 us -> 0 us
    psum x2 -> x0, waiting for transfers between devices: 137 us -> none  [sublayer(): preact = lax.psum(partial_value, 'ra')]
    psum x4 -> x0, blocking collectives: 63.1 us -> none  [the longest x2 42.8 us: sublayer(): squares = lax.psum(own_squares, 'ra')]
    pallas_call x0 -> x1, Pallas kernels: none -> 35.1 us  [local(): pl.pallas_call(functools.partial(kernel, n, m, cols * n), out_shape=jax.S...]
    dot_general x4 -> x0, matrix products: 5.2 us -> none  [the longest x2 2.96 us: sublayer(): partial_value = jnp.dot(normed, up_bf, preferred_element_type=jnp.float32)]
  transfers between devices with their start and end apart: 2 -> 0, of which waited for: 2 -> 0; matrix products, arithmetic and copies ran while one was open for 0% -> 0% of each run, Pallas kernels for 0% -> 0%
where the time goes in v1:
time: 36.7 us; the launch traced here: 36.4 us
  Pallas kernels  35.1 us (96%)
  local copies, waits for them, and re-layouts  1.32 us (4%)
    pallas_call x1, Pallas kernels, local(): pl.pallas_call(functools.partial(kernel, n, m, cols * n), out_shape=jax.S...  35.1 us
    unnamed x1, local copies, waits for them, and re-layouts  1.32 us

profile of v1, /device:TPU:0, one launch (start us, length us, event | category | flops | bytes accessed | tf_op | source)
XLA Modules:
  0.0 36.4 jit_solution(5701308388069020422)
XLA Ops:
  0.0 35.1 %shard_map.73 = bf16[64,128]{1,0:T(8,128)(2,1)} custom-call(bf16[64,128]{1,0:T(8,128)(2,1)} %stream_hbm.1, f32[1,128]{1,0:T(1,128)} %bitcast.2, f32[128,1024]{1,0:T(8,128)} %up1_hbm.1, f32[1024,128]{1,0:T(8,128)} %down1_hbm.1, f32[1,128]{1,0:T(1,128)} %bitcast.3, f32[128,1024]{1,0:T(8,128)} %up2_hbm.1, f32[1024,128]{1,0:T(8,128)} %down2_hbm.1), custom_call_target="tpu_custom_call" | custom-call | tf_op jit(solution)/shard_map/pallas_call | solution.py:170
  35.1 1.3 %copy.9 = bf16[64,128]{1,0:T(8,128)(2,1)} copy(bf16[64,128]{1,0:T(8,128)(2,1)} %shard_map.73) | data formatting | bytes 32768

commit v2 on v1

--- a/solution.py
+++ b/solution.py
@@ -20,7 +20,7 @@
     n, m, width,
     stream_hbm, gain1_hbm, up1_hbm, down1_hbm, gain2_hbm, up2_hbm, down2_hbm,
     out_ref,
-    stream_v, gain_v, up_v, down_v, down_b,
+    stream_v, gain_v, up_v, up_b, down_v, down_b,
     part_out, part_in, sq_out, sq_in, act, branch_in,
     load_sem, part_ss, part_rs, sq_ss, sq_rs, act_ss, act_rs, br_ss, br_rs,
 ):
@@ -29,8 +29,17 @@
     tokens = stream_v.shape[0]
     block = part_out.shape[-1]
 
+    pair = 2 if n % 2 == 0 else 1
+    half = lax.div(2 * ra, n)
+    own_group = half * lax.div(ra, pair) + (1 - half) * (n // pair - 1 - lax.div(ra, pair))
+    own_place = pair * own_group
+
     def ra_peer(step):
-        return lax.rem(ra + step, n)
+        place = step - 1
+        place = place + lax.div(place - own_place + n, n)
+        group = lax.div(place, pair)
+        group = half * group + (1 - half) * (n // pair - 1 - group)
+        return pair * group + lax.rem(ra + place, pair)
 
     def cb_peer(step):
         return lax.rem(cb + step, m)
@@ -74,12 +83,12 @@
     result = None
     for layer in range(2):
         scaled = (floated * gain_v[layer]).astype(BF16)
-        loads[2 + 3 * layer].wait()
-        partial = jnp.dot(scaled, up_v[layer].astype(BF16), preferred_element_type=F32)
+        if layer == 0:
+            loads[2].wait()
+        up = up_v[layer].astype(BF16) if layer == 0 else up_b[...]
+        partial = jnp.dot(scaled, up, preferred_element_type=F32)
         for j in range(n):
             part_out[layer, j] = partial[:, j * block:(j + 1) * block].astype(BF16)
-        own = jnp.sum(floated * floated, axis=1, keepdims=True)
-        sq_out[layer] = jnp.broadcast_to(own, (tokens, LANES)).T[:ROWS]
         if layer == 0:
             pl.semaphore_wait(barrier, n + m - 2)
         copies = []
@@ -88,6 +97,12 @@
             copies.append(to_ra(
                 part_out.at[layer, peer], part_in.at[layer, ra],
                 part_ss.at[layer, peer], part_rs.at[layer, ra], peer))
+        for copy in copies:
+            copy.start()
+        sends += copies
+        own = jnp.sum(floated * floated, axis=1, keepdims=True)
+        sq_out[layer] = jnp.broadcast_to(own, (tokens, LANES)).T[:ROWS]
+        copies = []
         for step in range(1, n):
             peer = ra_peer(step)
             copies.append(to_ra(
@@ -119,6 +134,10 @@
         for copy in copies:
             copy.start()
         sends += copies
+
+        if layer == 0:
+            loads[5].wait()
+            up_b[...] = up_v[1].astype(BF16)
 
         squares = sq_out[layer]
         for step in range(1, n):
@@ -176,6 +195,7 @@
             pltpu.VMEM((tokens, cols), BF16),
             pltpu.VMEM((2, 1, cols), F32),
             pltpu.VMEM((2, cols, hidden), F32),
+            pltpu.VMEM((cols, hidden), BF16),
             pltpu.VMEM((2, hidden, cols), F32),
             pltpu.VMEM((2, n, block, cols), BF16),
             pltpu.VMEM((2, n, tokens, block), BF16),

time: 36.7 us -> 35.3 us (0.962)
  Pallas kernels: 35.1 us -> 33.6 us
    pallas_call x1, Pallas kernels: 35.1 us -> 33.6 us  [local(): pl.pallas_call(functools.partial(kernel, n, m, cols * n), out_shape=jax.S...]
where the time goes in v2:
time: 35.3 us; the launch traced here: 35 us
  Pallas kernels  33.6 us (95%)
  local copies, waits for them, and re-layouts  1.32 us (4%)
    pallas_call x1, Pallas kernels, local(): pl.pallas_call(functools.partial(kernel, n, m, cols * n), out_shape=jax.S...  33.6 us
    unnamed x1, local copies, waits for them, and re-layouts  1.32 us

profile of v2, /device:TPU:0, one launch (start us, length us, event | category | flops | bytes accessed | tf_op | source)
XLA Modules:
  0.0 35.0 jit_solution(11761911703235533245)
XLA Ops:
  0.0 33.6 %shard_map.73 = bf16[64,128]{1,0:T(8,128)(2,1)} custom-call(bf16[64,128]{1,0:T(8,128)(2,1)} %stream_hbm.1, f32[1,128]{1,0:T(1,128)} %bitcast.2, f32[128,1024]{1,0:T(8,128)} %up1_hbm.1, f32[1024,128]{1,0:T(8,128)} %down1_hbm.1, f32[1,128]{1,0:T(1,128)} %bitcast.3, f32[128,1024]{1,0:T(8,128)} %up2_hbm.1, f32[1024,128]{1,0:T(8,128)} %down2_hbm.1), custom_call_target="tpu_custom_call" | custom-call | tf_op jit(solution)/shard_map/pallas_call | solution.py:189
  33.6 1.3 %copy.9 = bf16[64,128]{1,0:T(8,128)(2,1)} copy(bf16[64,128]{1,0:T(8,128)(2,1)} %shard_map.73) | data formatting | bytes 32768
